TPU v7x, 32 devices: a whole 2x2x4 slice. The times are simulated.
32 devices in a mesh: ep: 4 (over y, x), tp: 8 (over z, core).
Axes of the slice: x: 2, y: 2, z: 4, core: 2. Of those that a mesh axis runs over, the one named last changes fastest.
Arguments:
- tokens: bfloat16 [768, 2048], P('ep'), may hold values from -6 to 6
- cotangent: bfloat16 [768, 2048], P('ep'), may hold values from -6 to 6
- routes: int32 [768, 2], P('ep'), may hold values from 0 to 3, all different within a row; in each aligned block of 192 rows (0 to 191, 192 to 383, ...) at most 192 rows name the same one
- route_weight: float32 [768, 2], P('ep'), may hold values from 0.2 to 1
- gate_weight: bfloat16 [4, 2048, 4096], P('ep', None, 'tp'), may hold values from -0.125 to 0.125
- up_weight: bfloat16 [4, 2048, 4096], P('ep', None, 'tp'), may hold values from -0.125 to 0.125
- down_weight: bfloat16 [4, 4096, 2048], P('ep', 'tp'), may hold values from -0.09375 to 0.09375
Outputs:
- grad_tokens: bfloat16 [768, 2048], P('ep', 'tp')
- grad_route: float32 [768, 2], P('ep')
- grad_gate: bfloat16 [4, 2048, 4096], P('ep', None, 'tp')
- grad_up: bfloat16 [4, 2048, 4096], P('ep', None, 'tp')
- grad_down: bfloat16 [4, 4096, 2048], P('ep', 'tp')
Inputs may be any that keep to these rules, and one draw needn't show every extreme that they name: `routes`: within the rows of one device along ep, each expert is named at most 192 times, a bound that some block reaches; the 2 entries of a row differ.
All inputs are finite; a program needn't handle non-finite values.
Results may differ from a plain program's by a relative error of at most 0.025.
Values may be sent and summed in bfloat16 or wider, within the bound.
A program may use at most 64 MiB of HBM per device.

v0:
```python
import functools

import jax
import jax.numpy as jnp
from jax import lax
from jax.experimental import pallas as pl
from jax.experimental.pallas import tpu as pltpu
from jax.sharding import PartitionSpec as P

F32, BF16 = jnp.float32, jnp.bfloat16
LANES = 256
CHUNKS = 2
VLIM = 48


def shards(tokens, cotangent, routes, route_weight, gate_weight, up_weight, down_weight):
    rows, model_width = tokens.shape
    top = routes.shape[1]
    local_experts = gate_weight.shape[0]
    experts_all = local_experts * lax.axis_size("ep")
    capacity = 2 * rows * top // experts_all
    shard_width = model_width // lax.axis_size("tp")
    flat_routes = routes.reshape(-1)
    expert_ids = jnp.arange(experts_all, dtype=jnp.int32)
    onehot_table = (flat_routes[:, None] == expert_ids[None, :]).astype(jnp.int32)
    earlier = jnp.cumsum(onehot_table, axis=0) - onehot_table
    order_in = jnp.sum(earlier * onehot_table, axis=1)
    slot_index = flat_routes * capacity + order_in
    entries = jnp.arange(rows * top, dtype=jnp.int32) + 1
    slot_table = jnp.zeros((experts_all * capacity,), jnp.int32).at[slot_index].set(entries)
    filled = slot_table > 0
    entry = jnp.maximum(slot_table - 1, 0)
    source_row = entry // top
    zero_value = jnp.zeros((), jnp.bfloat16)
    token_buf = jnp.where(filled[:, None], tokens[source_row], zero_value).reshape(
        experts_all, capacity, model_width
    )
    cot_buf = jnp.where(filled[:, None], cotangent[source_row], zero_value).reshape(
        experts_all, capacity, model_width
    )
    weight_buf = (
        jnp.where(filled, route_weight.reshape(-1)[entry], 0.0)
        .astype(jnp.bfloat16)
        .reshape(experts_all, capacity)
    )
    start = lax.axis_index("tp") * shard_width
    token_part = lax.dynamic_slice_in_dim(token_buf, start, shard_width, 2)
    cot_part = lax.dynamic_slice_in_dim(cot_buf, start, shard_width, 2)
    token_part, cot_part, arrived_weight = (
        lax.all_to_all(token_part, "ep", split_axis=0, concat_axis=1, tiled=True),
        lax.all_to_all(cot_part, "ep", split_axis=0, concat_axis=1, tiled=True),
        lax.all_to_all(weight_buf, "ep", split_axis=0, concat_axis=1, tiled=True),
    )
    arrived_tokens, arrived_cot = (
        lax.all_gather(token_part, "tp", axis=2, tiled=True),
        lax.all_gather(cot_part, "tp", axis=2, tiled=True),
    )
    gate_pre = jnp.einsum(
        "erd,edf->erf", arrived_tokens, gate_weight, preferred_element_type=jnp.float32
    )
    up_pre = jnp.einsum(
        "erd,edf->erf", arrived_tokens, up_weight, preferred_element_type=jnp.float32
    )
    sig = jax.nn.sigmoid(gate_pre)
    active = gate_pre * sig
    hidden = (active * up_pre).astype(jnp.bfloat16)
    back_raw = jnp.einsum(
        "erd,efd->erf", arrived_cot, down_weight, preferred_element_type=jnp.float32
    )
    route_part = jnp.sum(hidden.astype(jnp.float32) * back_raw, axis=2)
    slot_weight = arrived_weight.astype(jnp.float32)
    scaled_back = slot_weight[:, :, None] * back_raw
    grad_gate_pre = (scaled_back * up_pre * sig * (1.0 + gate_pre * (1.0 - sig))).astype(
        jnp.bfloat16
    )
    grad_up_pre = (scaled_back * active).astype(jnp.bfloat16)
    scaled_cot = (slot_weight[:, :, None] * arrived_cot).astype(jnp.bfloat16)
    grad_gate = jnp.einsum(
        "erd,erf->edf", arrived_tokens, grad_gate_pre, preferred_element_type=jnp.float32
    ).astype(jnp.bfloat16)
    grad_up = jnp.einsum(
        "erd,erf->edf", arrived_tokens, grad_up_pre, preferred_element_type=jnp.float32
    ).astype(jnp.bfloat16)
    grad_down = jnp.einsum(
        "erf,erd->efd", hidden, scaled_cot, preferred_element_type=jnp.float32
    ).astype(jnp.bfloat16)
    row_part = jnp.einsum(
        "erf,edf->erd", grad_gate_pre, gate_weight, preferred_element_type=jnp.float32
    )
    row_part = row_part + jnp.einsum(
        "erf,edf->erd", grad_up_pre, up_weight, preferred_element_type=jnp.float32
    )
    row_summed = lax.psum_scatter(
        row_part.astype(jnp.bfloat16), "tp", scatter_dimension=2, tiled=True
    )
    returned = lax.all_to_all(row_summed, "ep", split_axis=1, concat_axis=0, tiled=True)
    route_total = lax.psum(route_part, "tp")
    route_back = lax.all_to_all(route_total, "ep", split_axis=1, concat_axis=0, tiled=True)
    per_entry = returned.reshape(experts_all * capacity, shard_width)[slot_index]
    grad_tokens = jnp.sum(
        per_entry.astype(jnp.float32).reshape(rows, top, shard_width), axis=1
    ).astype(jnp.bfloat16)
    grad_route = route_back.reshape(-1)[slot_index].reshape(rows, top)
    return (grad_tokens, grad_route, grad_gate, grad_up, grad_down)


def step_kernel(
    n_ep, n_tp,
    x_hbm, c_hbm, routes_ref, weight_ref, wg_hbm, wu_hbm, wd_hbm,
    gt_ref, rt_ref, gg, gu, gd,
    xc, wt, wg, wu, wd, hid, da, db, sc, rp, pr, r1, r2, zr, rcol, rm, rr, ra, rb,
    lsem, s_fwd, r_fwd, s_pair, r_pair, s_rp, r_rp, s_xy, r_xy, s_z, r_z, s_rt, r_rt,
):
    nz = n_tp // 2
    hz = nz // 2
    rows, width = x_hbm.shape
    hidden_units = wg.shape[1]
    shard = width // n_tp
    piece = rows // (nz + 2)
    unit = rows // CHUNKS
    p, t = lax.axis_index("ep"), lax.axis_index("tp")
    k, z = t % 2, t // 2
    px, py, pd = p + 1 - 2 * (p % 2), p + 2 - 4 * (p // 2), 3 - p
    mate = t + 1 - 2 * k

    def remote(src, dst, send, recv, ep, tp):
        return pltpu.make_async_remote_copy(
            src_ref=src, dst_ref=dst, send_sem=send, recv_sem=recv,
            device_id={"ep": ep, "tp": tp}, device_id_type=pl.DeviceIdType.MESH,
        )

    local = [
        pltpu.make_async_copy(x_hbm, xc.at[p, pl.ds(0, rows)], lsem.at[0]),
        pltpu.make_async_copy(c_hbm, xc.at[p, pl.ds(rows, rows)], lsem.at[1]),
        pltpu.make_async_copy(wg_hbm, wg, lsem.at[2]),
        pltpu.make_async_copy(wu_hbm, wu, lsem.at[3]),
        pltpu.make_async_copy(wd_hbm, wd, lsem.at[4]),
    ]
    for copy in local:
        copy.start()
    barrier = pltpu.get_barrier_semaphore()
    for other in (px, py, pd):
        pl.semaphore_signal(barrier, inc=1, device_id={"ep": other, "tp": t}, device_id_type=pl.DeviceIdType.MESH)
    for step in range(1, n_tp):
        pl.semaphore_signal(barrier, inc=1, device_id={"ep": p, "tp": (t + step) % n_tp}, device_id_type=pl.DeviceIdType.MESH)
    experts = lax.broadcasted_iota(jnp.int32, (8, rows), 0)
    mixed = jnp.zeros((8, rows), F32)
    for choice in range(routes_ref.shape[0]):
        hit = routes_ref[choice:choice + 1, :] == experts
        mixed = mixed + jnp.where(hit, weight_ref[choice:choice + 1, :], 0.0)
    wt[p] = jnp.zeros(wt.shape[1:], F32)
    wt[p, :, 0:rows] = mixed.astype(BF16).astype(F32)
    pl.semaphore_wait(barrier, n_ep - 1 + n_tp - 1)
    for copy in local[:2]:
        copy.wait()

    sends = []

    def go(copy):
        copy.start()
        sends.append(copy)

    def sub_rows(half, lower, count):
        return pl.ds(pl.multiple_of(half * rows + lower, 16), count)

    def piece_rows(half, owner):
        return sub_rows(half, (2 + owner) * piece, piece)

    def half_rows(half, chunk):
        return pl.ds(pl.multiple_of(half * rows + chunk * unit, 16), unit)

    for at, other in enumerate((pd, px, py)):
        go(remote(wt.at[p], wt.at[p], s_fwd.at[at], r_fwd.at[at], other, t))
    mine = xc.at[p, piece_rows(k, z)]
    go(remote(mine, mine, s_fwd.at[3], r_fwd.at[3], pd, t))
    for chunk in range(CHUNKS):
        for at, other in enumerate((px, py)):
            sem = 4 + 2 * chunk + at
            mine = xc.at[p, half_rows(k, chunk)]
            go(remote(mine, mine, s_fwd.at[sem], r_fwd.at[sem], other, t))

    def arrived(ref, send, recv):
        remote(ref, ref, send, recv, p, mate).wait_recv()

    mine = xc.at[pd, piece_rows(k, z)]
    arrived(mine, s_fwd.at[3], r_fwd.at[3])
    for step in range(1, nz):
        go(remote(mine, mine, s_z.at[step], r_z.at[step], p, (t + 2 * step) % n_tp))
    go(remote(mine, mine, s_pair.at[0], r_pair.at[0], p, mate))
    for copy in local[2:]:
        copy.wait()
    arrived(wt.at[pd], s_fwd.at[0], r_fwd.at[0])
    arrived(wt.at[px], s_fwd.at[1], r_fwd.at[1])
    arrived(wt.at[py], s_fwd.at[2], r_fwd.at[2])

    nt = (((1,), (1,)), ((), ()))
    tn = (((0,), (0,)), ((), ()))

    def weights_of(b):
        at_expert = lax.broadcasted_iota(jnp.int32, wt.shape[1:], 0) == p
        row = jnp.sum(jnp.where(at_expert, wt[b], 0.0), axis=0, keepdims=True)
        return jnp.broadcast_to(row, (128, LANES)).T[:, 0:1]

    def compute(parts):
        count = sum(size for _, _, size in parts)

        def load(ref, shift, cols):
            got = [ref[b, pl.ds(shift + lower, size), cols] for b, lower, size in parts]
            return got[0] if len(got) == 1 else jnp.concatenate(got, axis=0)

        def store(ref, cols, value):
            done = 0
            for b, lower, size in parts:
                ref[b, pl.ds(lower, size), cols] = value[done:done + size]
                done += size

        every = slice(None)
        weight = [weights_of(b)[lower:lower + size] for b, lower, size in parts]
        weight = weight[0] if len(weight) == 1 else jnp.concatenate(weight, axis=0)
        tile = min(hidden_units, 256)
        route = jnp.zeros((count, 1), F32)
        for at in range(hidden_units // tile):
            cols = pl.ds(at * tile, tile)
            x = load(xc, 0, every)
            gate = jnp.dot(x, wg[:, cols], preferred_element_type=F32)
            up = jnp.dot(x, wu[:, cols], preferred_element_type=F32)
            back = lax.dot_general(load(xc, rows, every), wd[cols, :], nt, preferred_element_type=F32)
            sig = jax.nn.sigmoid(gate)
            active = gate * sig
            hidden = (active * up).astype(BF16)
            store(hid, cols, hidden)
            route = route + jnp.sum(hidden.astype(F32) * back, axis=1, keepdims=True)
            scaled = weight * back
            store(da, cols, (scaled * up * sig * (1.0 + gate * (1.0 - sig))).astype(BF16))
            store(db, cols, (scaled * active).astype(BF16))
        store(rcol, every, jnp.broadcast_to(route, (count, 128)))
        for at in range(nz):
            cols = pl.ds(2 * at * shard, 2 * shard)
            part = lax.dot_general(load(da, 0, every), wg[cols, :], nt, preferred_element_type=F32)
            part = part + lax.dot_general(load(db, 0, every), wu[cols, :], nt, preferred_element_type=F32)
            part, done = part.astype(BF16), 0
            for b, lower, size in parts:
                for core in range(2):
                    rp[core, at, b, pl.ds(lower, size), :] = part[done:done + size, core * shard:(core + 1) * shard]
                done += size
        for b, lower, size in parts:
            for chunk in range(lower // unit, (lower + size) // unit):
                span = pl.ds(chunk * unit, unit)
                sem = CHUNKS * orders[id(b)] + chunk
                go(remote(rp.at[1 - k, :, b, span], pr.at[:, b, span], s_rp.at[sem], r_rp.at[sem], p, mate))
        store(sc, every, (weight * load(xc, rows, every).astype(F32)).astype(BF16))

    orders = {id(p): 0, id(px): 1, id(py): 2, id(pd): 3}
    def add_pair(b, chunk):
        span = pl.ds(chunk * unit, unit)
        sem = CHUNKS * orders[id(b)] + chunk
        arrived(pr.at[:, b, span], s_rp.at[sem], r_rp.at[sem])
        for at in range(nz):
            rp[k, at, b, span, :] = (rp[k, at, b, span, :].astype(F32) + pr[at, b, span, :].astype(F32)).astype(BF16)

    def xy_sem(at, kind, chunk):
        return (kind * nz + at) * CHUNKS + chunk

    def first(at, b, kind, other, chunk):
        span = pl.ds(chunk * unit, unit)
        sem = xy_sem(at, kind, chunk)
        go(remote(rp.at[k, at, b, span], r1.at[at, kind, span], s_xy.at[sem], r_xy.at[sem], other, t))

    def first_near(chunk):
        add_pair(px, chunk)
        add_pair(py, chunk)
        for at in range(hz):
            first(at, px, 0, px, chunk)
            first(hz + at, py, 0, py, chunk)

    compute([(p, 0, rows)])
    for chunk in range(CHUNKS):
        for at, other in enumerate((px, py)):
            mine = xc.at[other, half_rows(k, chunk)]
            sem = 4 + 2 * chunk + at
            arrived(mine, s_fwd.at[sem], r_fwd.at[sem])
            go(remote(mine, mine, s_pair.at[sem], r_pair.at[sem], p, mate))
            if chunk == 0:
                passed = xc.at[other, sub_rows(k, at * piece, piece)]
                sem = 4 + 2 * CHUNKS + at
                go(remote(passed, passed, s_fwd.at[sem], r_fwd.at[sem], py if at == 0 else px, t))
        if chunk == CHUNKS - 1:
            for step in range(1, nz):
                mine = xc.at[pd, piece_rows(k, (z - step + nz) % nz)]
                arrived(mine, s_z.at[step], r_z.at[step])
                go(remote(mine, mine, s_pair.at[step], r_pair.at[step], p, mate))
        for at, other in enumerate((px, py)):
            sem = 4 + 2 * chunk + at
            arrived(xc.at[other, half_rows(1 - k, chunk)], s_pair.at[sem], r_pair.at[sem])
        compute([(px, chunk * unit, unit), (py, chunk * unit, unit)])
        if chunk == 0:
            add_pair(p, 0)
            add_pair(p, 1)
    for at in range(2):
        sem = 4 + 2 * CHUNKS + at
        passed = xc.at[pd, sub_rows(k, at * piece, piece)]
        arrived(passed, s_fwd.at[sem], r_fwd.at[sem])
        go(remote(passed, passed, s_pair.at[sem], r_pair.at[sem], p, mate))
    for chunk in range(CHUNKS):
        first_near(chunk)
    for at in range(2):
        sem = 4 + 2 * CHUNKS + at
        arrived(xc.at[pd, sub_rows(1 - k, at * piece, piece)], s_pair.at[sem], r_pair.at[sem])
    for step in range(nz):
        arrived(xc.at[pd, piece_rows(1 - k, (z - step + nz) % nz)], s_pair.at[step], r_pair.at[step])
    compute([(pd, 0, rows)])
    for chunk in range(CHUNKS):
        add_pair(pd, chunk)
        for at in range(hz):
            first(at, pd, 1, px, chunk)
            first(hz + at, pd, 1, py, chunk)

    for b in range(n_ep):
        rm[b:b + 1, :] = rcol[b].T[0:1, :]
    for step in range(1, n_tp):
        go(remote(rm, rr.at[step], s_rt.at[step], r_rt.at[step], p, (t + step) % n_tp))

    def wide(ref, lower, count, cols):
        got = ref[:, pl.ds(lower, count), cols]
        return got.reshape(n_ep * count, got.shape[2])

    def weight_grad(grads, out):
        @pl.loop(0, width // 256)
        def _(at):
            cols = pl.ds(pl.multiple_of(at * 256, 256), 256)
            out[cols, :] = lax.dot_general(
                wide(xc, 0, rows, cols), wide(grads, 0, rows, slice(None)), tn, preferred_element_type=F32
            ).astype(BF16)

    def second(at, b, other, chunk):
        span = pl.ds(chunk * unit, unit)
        sem = xy_sem(at, 1, chunk)
        arrived(r1.at[at, 1, span], s_xy.at[sem], r_xy.at[sem])
        rp[k, at, b, span, :] = (rp[k, at, b, span, :].astype(F32) + r1[at, 1, span, :].astype(F32)).astype(BF16)
        sem = xy_sem(at, 2, chunk)
        go(remote(rp.at[k, at, b, span], r2.at[at, span], s_xy.at[sem], r_xy.at[sem], other, t))

    def third(chunk):
        span = pl.ds(chunk * unit, unit)
        for at in range(nz):
            for kind, ref in ((0, r1.at[at, 0, span]), (2, r2.at[at, span])):
                sem = xy_sem(at, kind, chunk)
                arrived(ref, s_xy.at[sem], r_xy.at[sem])
            mine = rp[k, at, p, span, :].astype(F32) + r1[at, 0, span, :].astype(F32) + r2[at, span, :].astype(F32)
            rp[k, at, p, span, :] = mine.astype(BF16)
        for step in range(1, nz):
            sem = (1 + chunk) * nz + step
            go(remote(rp.at[k, (z + step) % nz, p, span], zr.at[step, span], s_z.at[sem], r_z.at[sem], p, (t + 2 * step) % n_tp))

    for chunk in range(CHUNKS):
        for at in range(hz):
            second(at, py, py, chunk)
            second(hz + at, px, px, chunk)

    total = rm[...]
    for step in range(1, n_tp):
        arrived(rr.at[step], s_rt.at[step], r_rt.at[step])
        total = total + rr[step]
    ra[...] = total
    for at, other in enumerate((px, py, pd)):
        go(remote(ra, rb.at[at], s_rt.at[n_tp + at], r_rt.at[n_tp + at], other, t))

    weight_grad(da, gg)
    third(0)
    weight_grad(db, gu)
    third(1)

    @pl.loop(0, hidden_units // 256)
    def _(at):
        units = pl.ds(pl.multiple_of(at * 256, 256), 256)
        left = wide(hid, 0, rows, units)

        @pl.loop(0, width // 512)
        def _(to):
            cols = pl.ds(pl.multiple_of(to * 512, 512), 512)
            gd[units, cols] = lax.dot_general(
                left, wide(sc, 0, rows, cols), tn, preferred_element_type=F32
            ).astype(BF16)

    index = lax.broadcasted_iota(jnp.int32, rm.shape, 0)
    result = jnp.zeros(rm.shape, F32)
    for at, other in enumerate((px, py, pd, p)):
        if at < 3:
            arrived(rb.at[at], s_rt.at[n_tp + at], r_rt.at[n_tp + at])
        got = rb[at] if at < 3 else ra[...]
        row = jnp.sum(jnp.where(index == p, got, 0.0), axis=0, keepdims=True)
        result = result + jnp.where(index == other, row, 0.0)
    for choice in range(routes_ref.shape[0]):
        hit = routes_ref[choice:choice + 1, :] == experts
        rt_ref[choice:choice + 1, :] = jnp.sum(jnp.where(hit, result[:, 0:rows], 0.0), axis=0, keepdims=True)

    total = rp[k, z, p].astype(F32)
    for step in range(1, nz):
        for chunk in range(CHUNKS):
            sem = (1 + chunk) * nz + step
            arrived(zr.at[step, pl.ds(chunk * unit, unit)], s_z.at[sem], r_z.at[sem])
        total = total + zr[step].astype(F32)
    gt_ref[...] = total.astype(BF16)
    for copy in sends:
        copy.wait_send()


def fused(n_ep, n_tp, tokens, cotangent, routes, route_weight, gate_weight, up_weight, down_weight):
    rows, width = tokens.shape
    units = gate_weight.shape[2]
    nz = n_tp // 2
    shard = width // n_tp
    hbm, vmem = pl.BlockSpec(memory_space=pltpu.HBM), pl.BlockSpec(memory_space=pltpu.VMEM)
    dma = pltpu.SemaphoreType.DMA
    grad_tokens, by_choice, grad_gate, grad_up, grad_down = pl.pallas_call(
        functools.partial(step_kernel, n_ep, n_tp),
        out_shape=(
            jax.ShapeDtypeStruct((rows, shard), BF16),
            jax.ShapeDtypeStruct((routes.shape[1], rows), F32),
            jax.ShapeDtypeStruct((width, units), BF16),
            jax.ShapeDtypeStruct((width, units), BF16),
            jax.ShapeDtypeStruct((units, width), BF16),
        ),
        in_specs=[hbm, hbm, vmem, vmem, hbm, hbm, hbm],
        out_specs=(vmem,) * 5,
        scratch_shapes=[
            pltpu.VMEM((n_ep, 2 * rows, width), BF16),
            pltpu.VMEM((n_ep, 8, LANES), F32),
            pltpu.VMEM((width, units), BF16),
            pltpu.VMEM((width, units), BF16),
            pltpu.VMEM((units, width), BF16),
            pltpu.VMEM((n_ep, rows, units), BF16),
            pltpu.VMEM((n_ep, rows, units), BF16),
            pltpu.VMEM((n_ep, rows, units), BF16),
            pltpu.VMEM((n_ep, rows, width), BF16),
            pltpu.VMEM((2, nz, n_ep, rows, shard), BF16),
            pltpu.VMEM((nz, n_ep, rows, shard), BF16),
            pltpu.VMEM((nz, 2, rows, shard), BF16),
            pltpu.VMEM((nz, rows, shard), BF16),
            pltpu.VMEM((nz, rows, shard), BF16),
            pltpu.VMEM((n_ep, LANES, 128), F32),
            pltpu.VMEM((8, LANES), F32),
            pltpu.VMEM((n_tp, 8, LANES), F32),
            pltpu.VMEM((8, LANES), F32),
            pltpu.VMEM((3, 8, LANES), F32),
            dma((6,)),
            dma((6 + 2 * CHUNKS,)),
            dma((6 + 2 * CHUNKS,)),
            dma((6 + 2 * CHUNKS,)),
            dma((6 + 2 * CHUNKS,)),
            dma((n_ep * CHUNKS,)),
            dma((n_ep * CHUNKS,)),
            dma((3 * nz * CHUNKS,)),
            dma((3 * nz * CHUNKS,)),
            dma(((1 + CHUNKS) * nz,)),
            dma(((1 + CHUNKS) * nz,)),
            dma((n_tp + 3,)),
            dma((n_tp + 3,)),
        ],
        compiler_params=pltpu.CompilerParams(
            collective_id=0, has_side_effects=True, vmem_limit_bytes=VLIM * 1024 * 1024
        ),
    )(tokens, cotangent, routes.T, route_weight.T, gate_weight[0], up_weight[0], down_weight[0])
    grad_route = by_choice.T
    return grad_tokens, grad_route, grad_gate[None], grad_up[None], grad_down[None]


def body(mesh, *arrays):
    n_ep, n_tp = mesh.shape["ep"], mesh.shape["tp"]
    rows, width = arrays[0].shape
    experts, _, units = arrays[4].shape
    capacity = 2 * rows * arrays[2].shape[1] // (experts * n_ep)
    fits = (
        n_ep == 4 and experts == 1 and n_tp == 8 and capacity >= rows and rows <= LANES
        and width % (n_tp * 128) == 0 and width % 512 == 0 and units % 256 == 0
        and rows % (16 * (n_tp // 2 + 2)) == 0 and 2 * (rows // (n_tp // 2 + 2)) <= rows // CHUNKS and rows % (16 * CHUNKS) == 0
    )
    return fused(n_ep, n_tp, *arrays) if fits else shards(*arrays)


def solution(mesh):
    return jax.shard_map(
        functools.partial(body, mesh),
        mesh=mesh,
        in_specs=(
            P("ep", None),
            P("ep", None),
            P("ep", None),
            P("ep", None),
            P("ep", None, "tp"),
            P("ep", None, "tp"),
            P("ep", "tp", None),
        ),
        out_specs=(
            P("ep", "tp"),
            P("ep", None),
            P("ep", None, "tp"),
            P("ep", None, "tp"),
            P("ep", "tp", None),
        ),
        check_vma=False,
    )
```

profile of v0, /device:TPU:0, one launch (start us, length us, event | category | flops | bytes accessed | tf_op | source)
XLA Modules:
  0.0 71.3 jit_solution(18282407283631308743)
XLA Ops:
  0.6 0.0 copy-start
  0.6 1.1 %copy-done = bf16[192,2048]{1,0:T(8,128)(2,1)S(1)} copy-done((bf16[192,2048]{1,0:T(8,128)(2,1)S(1)}, bf16[192,2048]{1,0:T(8,128)(2,1)}, u32[]{:S(2)}) %copy-start) | copy-done | bytes 786456
  1.8 0.0 copy-start.1
  1.8 1.1 %copy-done.1 = bf16[192,2048]{1,0:T(8,128)(2,1)S(1)} copy-done((bf16[192,2048]{1,0:T(8,128)(2,1)S(1)}, bf16[192,2048]{1,0:T(8,128)(2,1)}, u32[]{:S(2)}) %copy-start.1) | copy-done | bytes 786456
  2.9 0.0 copy-start.2
  2.9 0.7 copy-done.2
  3.6 0.0 copy-start.3
  3.6 0.7 copy-done.3
  4.3 60.8 %shard_map.110 = (bf16[192,256]{1,0:T(8,128)(2,1)S(1)}, f32[2,192]{1,0:T(2,128)S(1)}, bf16[2048,512]{1,0:T(8,128)(2,1)S(1)}, bf16[2048,512]{1,0:T(8,128)(2,1)S(1)}, bf16[512,2048]{1,0:T(8,128)(2,1)}) custom-call(bf16[192,2048]{1,0:T(8,128)(2,1)S(1)} %copy-done, bf16[192,2048]{1,0:T(8,128)(2,1)S(1)} %copy-done.1, s32[2,192]{1,0:T(2,128)S(1)} %bitcast.11, ...), custom_call_target="tpu_custom_call" | custom-call | tf_op jit(solution)/shard_map/pallas_call | solution.py:415
  65.1 0.6 copy.17
  65.8 0.6 copy.18
  66.3 1.3 %copy.19 = bf16[1,2048,512]{2,1,0:T(8,128)(2,1)} copy(bf16[1,2048,512]{2,1,0:T(8,128)(2,1)S(1)} %bitcast.10) | data formatting | bytes 4194304
  67.6 0.0 copy-start.4
  67.7 1.3 %copy.20 = bf16[1,2048,512]{2,1,0:T(8,128)(2,1)} copy(bf16[1,2048,512]{2,1,0:T(8,128)(2,1)S(1)} %bitcast.9) | data formatting | bytes 4194304
  69.0 1.0 %copy-done.4 = bf16[512,2048]{1,0:T(8,128)(2,1)S(1)} copy-done((bf16[512,2048]{1,0:T(8,128)(2,1)S(1)}, bf16[512,2048]{1,0:T(8,128)(2,1)}, u32[]{:S(2)}) %copy-start.4) | copy-done | bytes 2097176
  70.0 1.3 %copy.21 = bf16[1,512,2048]{2,1,0:T(8,128)(2,1)} copy(bf16[1,512,2048]{2,1,0:T(8,128)(2,1)S(1)} %bitcast.17) | data formatting | bytes 4194304
Async XLA Ops:
  0.6 1.1 %copy-start = (bf16[192,2048]{1,0:T(8,128)(2,1)S(1)}, bf16[192,2048]{1,0:T(8,128)(2,1)}, u32[]{:S(2)}) copy-start(bf16[192,2048]{1,0:T(8,128)(2,1)} %x_hbm.1) | copy-start | bytes 2359300
  1.8 1.1 %copy-start.1 = (bf16[192,2048]{1,0:T(8,128)(2,1)S(1)}, bf16[192,2048]{1,0:T(8,128)(2,1)}, u32[]{:S(2)}) copy-start(bf16[192,2048]{1,0:T(8,128)(2,1)} %c_hbm.1) | copy-start | bytes 2359300
  2.9 0.7 copy-start.2
  3.6 0.7 copy-start.3
  67.6 2.3 %copy-start.4 = (bf16[512,2048]{1,0:T(8,128)(2,1)S(1)}, bf16[512,2048]{1,0:T(8,128)(2,1)}, u32[]{:S(2)}) copy-start(bf16[512,2048]{1,0:T(8,128)(2,1)} %get-tuple-element.14) | copy-start | bytes 6291460
where the time goes:
time: 71.7 us; the launch traced here: 71.3 us
  Pallas kernels  60.8 us (85%)
  local copies, waits for them, and re-layouts  9.83 us (14%)
    pallas_call x1, Pallas kernels, fused(): pl.pallas_call(functools.partial(step_kernel, n_ep, n_tp), out_shape=(jax...  60.8 us
    unnamed x15, local copies, waits for them, and re-layouts  9.83 us

commit v1 on v0

--- a/solution.py
+++ b/solution.py
@@ -10,7 +10,7 @@
 F32, BF16 = jnp.float32, jnp.bfloat16
 LANES = 256
 CHUNKS = 2
-VLIM = 48
+VLIM = 40
 
 
 def shards(tokens, cotangent, routes, route_weight, gate_weight, up_weight, down_weight):
@@ -106,9 +106,9 @@
 
 def step_kernel(
     n_ep, n_tp,
-    x_hbm, c_hbm, routes_ref, weight_ref, wg_hbm, wu_hbm, wd_hbm,
+    x_hbm, c_hbm, routes_hbm, weight_hbm, wg_hbm, wu_hbm, wd_hbm,
     gt_ref, rt_ref, gg, gu, gd,
-    xc, wt, wg, wu, wd, hid, da, db, sc, rp, pr, r1, r2, zr, rcol, rm, rr, ra, rb,
+    routes_ref, weight_ref, xc, wt, wg, wu, wd, hid, da, db, sc, rp, pr, r1, r2, zr, rcol, rm, rr, ra, rb,
     lsem, s_fwd, r_fwd, s_pair, r_pair, s_rp, r_rp, s_xy, r_xy, s_z, r_z, s_rt, r_rt,
 ):
     nz = n_tp // 2
@@ -132,6 +132,8 @@
     local = [
         pltpu.make_async_copy(x_hbm, xc.at[p, pl.ds(0, rows)], lsem.at[0]),
         pltpu.make_async_copy(c_hbm, xc.at[p, pl.ds(rows, rows)], lsem.at[1]),
+        pltpu.make_async_copy(routes_hbm, routes_ref, lsem.at[5]),
+        pltpu.make_async_copy(weight_hbm, weight_ref, lsem.at[6]),
         pltpu.make_async_copy(wg_hbm, wg, lsem.at[2]),
         pltpu.make_async_copy(wu_hbm, wu, lsem.at[3]),
         pltpu.make_async_copy(wd_hbm, wd, lsem.at[4]),
@@ -143,6 +145,8 @@
         pl.semaphore_signal(barrier, inc=1, device_id={"ep": other, "tp": t}, device_id_type=pl.DeviceIdType.MESH)
     for step in range(1, n_tp):
         pl.semaphore_signal(barrier, inc=1, device_id={"ep": p, "tp": (t + step) % n_tp}, device_id_type=pl.DeviceIdType.MESH)
+    for copy in local[2:4]:
+        copy.wait()
     experts = lax.broadcasted_iota(jnp.int32, (8, rows), 0)
     mixed = jnp.zeros((8, rows), F32)
     for choice in range(routes_ref.shape[0]):
@@ -187,7 +191,7 @@
     for step in range(1, nz):
         go(remote(mine, mine, s_z.at[step], r_z.at[step], p, (t + 2 * step) % n_tp))
     go(remote(mine, mine, s_pair.at[0], r_pair.at[0], p, mate))
-    for copy in local[2:]:
+    for copy in local[4:]:
         copy.wait()
     arrived(wt.at[pd], s_fwd.at[0], r_fwd.at[0])
     arrived(wt.at[px], s_fwd.at[1], r_fwd.at[1])
@@ -405,6 +409,15 @@
         copy.wait_send()
 
 
+def write_kernel(*refs):
+    sem = refs[-1]
+    copies = [pltpu.make_async_copy(refs[at], refs[5 + at], sem.at[at]) for at in range(5)]
+    for copy in copies:
+        copy.start()
+    for copy in copies:
+        copy.wait()
+
+
 def fused(n_ep, n_tp, tokens, cotangent, routes, route_weight, gate_weight, up_weight, down_weight):
     rows, width = tokens.shape
     units = gate_weight.shape[2]
@@ -421,9 +434,11 @@
             jax.ShapeDtypeStruct((width, units), BF16),
             jax.ShapeDtypeStruct((units, width), BF16),
         ),
-        in_specs=[hbm, hbm, vmem, vmem, hbm, hbm, hbm],
+        in_specs=[hbm] * 7,
         out_specs=(vmem,) * 5,
         scratch_shapes=[
+            pltpu.VMEM((routes.shape[1], rows), jnp.int32),
+            pltpu.VMEM((routes.shape[1], rows), F32),
             pltpu.VMEM((n_ep, 2 * rows, width), BF16),
             pltpu.VMEM((n_ep, 8, LANES), F32),
             pltpu.VMEM((width, units), BF16),
@@ -443,7 +458,7 @@
             pltpu.VMEM((n_tp, 8, LANES), F32),
             pltpu.VMEM((8, LANES), F32),
             pltpu.VMEM((3, 8, LANES), F32),
-            dma((6,)),
+            dma((7,)),
             dma((6 + 2 * CHUNKS,)),
             dma((6 + 2 * CHUNKS,)),
             dma((6 + 2 * CHUNKS,)),
@@ -460,7 +475,18 @@
         compiler_params=pltpu.CompilerParams(
             collective_id=0, has_side_effects=True, vmem_limit_bytes=VLIM * 1024 * 1024
         ),
-    )(tokens, cotangent, routes.T, route_weight.T, gate_weight[0], up_weight[0], down_weight[0])
+    )(*(pltpu.with_memory_space_constraint(array, pltpu.HBM) for array in (
+        tokens, cotangent, routes.T, route_weight.T, gate_weight[0], up_weight[0], down_weight[0]
+    )))
+    results = (grad_tokens, by_choice, grad_gate, grad_up, grad_down)
+    grad_tokens, by_choice, grad_gate, grad_up, grad_down = pl.pallas_call(
+        write_kernel,
+        out_shape=tuple(jax.ShapeDtypeStruct(array.shape, array.dtype) for array in results),
+        in_specs=[vmem] * 5,
+        out_specs=(hbm,) * 5,
+        scratch_shapes=[dma((5,))],
+        compiler_params=pltpu.CompilerParams(vmem_limit_bytes=1024 * 1024),
+    )(*results)
     grad_route = by_choice.T
     return grad_tokens, grad_route, grad_gate[None], grad_up[None], grad_down[None]
 

time: 71.7 us -> 63.3 us (0.88)
  local copies, waits for them, and re-layouts: 9.83 us -> 0 us
  Pallas kernels: 60.8 us -> 62.4 us
    unnamed x15 -> x0, local copies, waits for them, and re-layouts: 9.83 us -> none
    pallas_call x0 -> x1, Pallas kernels: none -> 2.78 us  [fused(): pl.pallas_call(write_kernel, out_shape=tuple((jax.ShapeDtypeStruct(array....]
    pallas_call x1, Pallas kernels: 60.8 us -> 59.6 us  [fused(): pl.pallas_call(functools.partial(step_kernel, n_ep, n_tp), out_shape=(jax...]
where the time goes in v1:
time: 63.3 us; the launch traced here: 63.1 us
  Pallas kernels  62.4 us (99%)
  between operations  0.64 us (1%)
    pallas_call x1, Pallas kernels, fused(): pl.pallas_call(functools.partial(step_kernel, n_ep, n_tp), out_shape=(jax...  59.6 us
    pallas_call x1, Pallas kernels, fused(): pl.pallas_call(write_kernel, out_shape=tuple((jax.ShapeDtypeStruct(array....  2.78 us

profile of v1, /device:TPU:0, one launch (start us, length us, event | category | flops | bytes accessed | tf_op | source)
XLA Modules:
  0.0 63.1 jit_solution(6789807531430817276)
XLA Ops:
  0.6 59.6 %shard_map.110 = (bf16[192,256]{1,0:T(8,128)(2,1)S(1)}, f32[2,192]{1,0:T(2,128)S(1)}, bf16[2048,512]{1,0:T(8,128)(2,1)S(1)}, bf16[2048,512]{1,0:T(8,128)(2,1)S(1)}, bf16[512,2048]{1,0:T(8,128)(2,1)S(1)}) custom-call(bf16[192,2048]{1,0:T(8,128)(2,1)} %x_hbm.1, bf16[192,2048]{1,0:T(8,128)(2,1)} %c_hbm.1, s32[2,192]{1,0:T(2,128)} %bitcast.12, ...), custom_call_target="tpu_custom_call" | custom-call | tf_op jit(solution)/shard_map/pallas_call | solution.py:428
  60.3 2.8 %shard_map.111 = (bf16[192,256]{1,0:T(8,128)(2,1)}, f32[2,192]{1,0:T(2,128)}, bf16[2048,512]{1,0:T(8,128)(2,1)}, bf16[2048,512]{1,0:T(8,128)(2,1)}, bf16[512,2048]{1,0:T(8,128)(2,1)}) custom-call(bf16[192,256]{1,0:T(8,128)(2,1)S(1)} %get-tuple-element.15.refs_0_, f32[2,192]{1,0:T(2,128)S(1)} %get-tuple-element.16.refs_1_, ...), custom_call_target="tpu_custom_call" | custom-call | tf_op jit(solution)/shard_map/pallas_call | solution.py:482

commit v2 on v1

--- a/solution.py
+++ b/solution.py
@@ -9,7 +9,8 @@
 
 F32, BF16 = jnp.float32, jnp.bfloat16
 LANES = 256
-CHUNKS = 2
+CHUNKS = 3
+PARTS = 4
 VLIM = 40
 
 
@@ -108,8 +109,8 @@
     n_ep, n_tp,
     x_hbm, c_hbm, routes_hbm, weight_hbm, wg_hbm, wu_hbm, wd_hbm,
     gt_ref, rt_ref, gg, gu, gd,
-    routes_ref, weight_ref, xc, wt, wg, wu, wd, hid, da, db, sc, rp, pr, r1, r2, zr, rcol, rm, rr, ra, rb,
-    lsem, s_fwd, r_fwd, s_pair, r_pair, s_rp, r_rp, s_xy, r_xy, s_z, r_z, s_rt, r_rt,
+    routes_ref, weight_ref, wgt, wut, wdt, xc, wt, wg, wu, wd, hid, da, db, sc, rp, pr, r1, r2, zr, rcol, rm, rr, ra, rb,
+    zq, rq, s_zf, r_zf, s_rq, r_rq, lsem, s_fwd, r_fwd, s_pair, r_pair, s_rp, r_rp, s_xy, r_xy, s_z, r_z, s_rt, r_rt,
 ):
     nz = n_tp // 2
     hz = nz // 2
@@ -117,7 +118,9 @@
     hidden_units = wg.shape[1]
     shard = width // n_tp
     piece = rows // (nz + 2)
-    unit = rows // CHUNKS
+    cuts = (0, 2 * piece, rows - piece, rows)
+    middle = 2 * piece + (rows - 3 * piece) // 32 * 16
+    ends = (0, 2 * piece, middle, rows - piece, rows)
     p, t = lax.axis_index("ep"), lax.axis_index("tp")
     k, z = t % 2, t // 2
     px, py, pd = p + 1 - 2 * (p % 2), p + 2 - 4 * (p // 2), 3 - p
@@ -170,34 +173,31 @@
     def piece_rows(half, owner):
         return sub_rows(half, (2 + owner) * piece, piece)
 
-    def half_rows(half, chunk):
-        return pl.ds(pl.multiple_of(half * rows + chunk * unit, 16), unit)
+    def half_rows(half, part):
+        return sub_rows(half, ends[part], ends[part + 1] - ends[part])
+
+    def span_of(chunk):
+        return pl.ds(cuts[chunk], cuts[chunk + 1] - cuts[chunk])
 
     for at, other in enumerate((pd, px, py)):
         go(remote(wt.at[p], wt.at[p], s_fwd.at[at], r_fwd.at[at], other, t))
     mine = xc.at[p, piece_rows(k, z)]
     go(remote(mine, mine, s_fwd.at[3], r_fwd.at[3], pd, t))
-    for chunk in range(CHUNKS):
+
+    def send_near(part):
         for at, other in enumerate((px, py)):
-            sem = 4 + 2 * chunk + at
-            mine = xc.at[p, half_rows(k, chunk)]
+            sem = 4 + 2 * part + at
+            mine = xc.at[p, half_rows(k, part)]
             go(remote(mine, mine, s_fwd.at[sem], r_fwd.at[sem], other, t))
+
+    send_near(0)
+    send_near(1)
 
     def arrived(ref, send, recv):
         remote(ref, ref, send, recv, p, mate).wait_recv()
 
-    mine = xc.at[pd, piece_rows(k, z)]
-    arrived(mine, s_fwd.at[3], r_fwd.at[3])
-    for step in range(1, nz):
-        go(remote(mine, mine, s_z.at[step], r_z.at[step], p, (t + 2 * step) % n_tp))
-    go(remote(mine, mine, s_pair.at[0], r_pair.at[0], p, mate))
     for copy in local[4:]:
         copy.wait()
-    arrived(wt.at[pd], s_fwd.at[0], r_fwd.at[0])
-    arrived(wt.at[px], s_fwd.at[1], r_fwd.at[1])
-    arrived(wt.at[py], s_fwd.at[2], r_fwd.at[2])
-
-    nt = (((1,), (1,)), ((), ()))
     tn = (((0,), (0,)), ((), ()))
 
     def weights_of(b):
@@ -228,7 +228,7 @@
             x = load(xc, 0, every)
             gate = jnp.dot(x, wg[:, cols], preferred_element_type=F32)
             up = jnp.dot(x, wu[:, cols], preferred_element_type=F32)
-            back = lax.dot_general(load(xc, rows, every), wd[cols, :], nt, preferred_element_type=F32)
+            back = jnp.dot(load(xc, rows, every), wdt[:, cols], preferred_element_type=F32)
             sig = jax.nn.sigmoid(gate)
             active = gate * sig
             hidden = (active * up).astype(BF16)
@@ -240,33 +240,55 @@
         store(rcol, every, jnp.broadcast_to(route, (count, 128)))
         for at in range(nz):
             cols = pl.ds(2 * at * shard, 2 * shard)
-            part = lax.dot_general(load(da, 0, every), wg[cols, :], nt, preferred_element_type=F32)
-            part = part + lax.dot_general(load(db, 0, every), wu[cols, :], nt, preferred_element_type=F32)
+            part = jnp.dot(load(da, 0, every), wgt[:, cols], preferred_element_type=F32)
+            part = part + jnp.dot(load(db, 0, every), wut[:, cols], preferred_element_type=F32)
             part, done = part.astype(BF16), 0
             for b, lower, size in parts:
                 for core in range(2):
                     rp[core, at, b, pl.ds(lower, size), :] = part[done:done + size, core * shard:(core + 1) * shard]
                 done += size
         for b, lower, size in parts:
-            for chunk in range(lower // unit, (lower + size) // unit):
-                span = pl.ds(chunk * unit, unit)
+            for chunk in range(CHUNKS):
+                if not lower <= cuts[chunk] < lower + size:
+                    continue
+                span = span_of(chunk)
                 sem = CHUNKS * orders[id(b)] + chunk
                 go(remote(rp.at[1 - k, :, b, span], pr.at[:, b, span], s_rp.at[sem], r_rp.at[sem], p, mate))
         store(sc, every, (weight * load(xc, rows, every).astype(F32)).astype(BF16))
 
     orders = {id(p): 0, id(px): 1, id(py): 2, id(pd): 3}
     def add_pair(b, chunk):
-        span = pl.ds(chunk * unit, unit)
+        span = span_of(chunk)
         sem = CHUNKS * orders[id(b)] + chunk
         arrived(pr.at[:, b, span], s_rp.at[sem], r_rp.at[sem])
         for at in range(nz):
             rp[k, at, b, span, :] = (rp[k, at, b, span, :].astype(F32) + pr[at, b, span, :].astype(F32)).astype(BF16)
 
+    def z_first(b):
+        add_pair(b, 0)
+        for step in range(1, nz):
+            sem = orders[id(b)] * nz + step
+            go(remote(
+                rp.at[k, (z + step) % nz, b, span_of(0)], zq.at[step, orders[id(b)]],
+                s_zf.at[sem], r_zf.at[sem], p, (t + 2 * step) % n_tp,
+            ))
+
+    def z_sum(b):
+        at, span = orders[id(b)], span_of(0)
+        total = rp[k, z, b, span, :].astype(F32)
+        for step in range(1, nz):
+            sem = at * nz + step
+            arrived(zq.at[step, at], s_zf.at[sem], r_zf.at[sem])
+            total = total + zq[step, at].astype(F32)
+        rp[k, z, b, span, :] = total.astype(BF16)
+        if at:
+            go(remote(rp.at[k, z, b, span], rq.at[at - 1], s_rq.at[at - 1], r_rq.at[at - 1], b, t))
+
     def xy_sem(at, kind, chunk):
         return (kind * nz + at) * CHUNKS + chunk
 
     def first(at, b, kind, other, chunk):
-        span = pl.ds(chunk * unit, unit)
+        span = span_of(chunk)
         sem = xy_sem(at, kind, chunk)
         go(remote(rp.at[k, at, b, span], r1.at[at, kind, span], s_xy.at[sem], r_xy.at[sem], other, t))
 
@@ -277,67 +299,110 @@
             first(at, px, 0, px, chunk)
             first(hz + at, py, 0, py, chunk)
 
-    compute([(p, 0, rows)])
-    for chunk in range(CHUNKS):
+    def first_pd(chunks):
+        for chunk in chunks:
+            add_pair(pd, chunk)
+            for at in range(hz):
+                first(at, pd, 1, px, chunk)
+                first(hz + at, pd, 1, py, chunk)
+
+    def take_near(part):
         for at, other in enumerate((px, py)):
-            mine = xc.at[other, half_rows(k, chunk)]
-            sem = 4 + 2 * chunk + at
+            mine = xc.at[other, half_rows(k, part)]
+            sem = 4 + 2 * part + at
             arrived(mine, s_fwd.at[sem], r_fwd.at[sem])
             go(remote(mine, mine, s_pair.at[sem], r_pair.at[sem], p, mate))
-            if chunk == 0:
-                passed = xc.at[other, sub_rows(k, at * piece, piece)]
-                sem = 4 + 2 * CHUNKS + at
-                go(remote(passed, passed, s_fwd.at[sem], r_fwd.at[sem], py if at == 0 else px, t))
-        if chunk == CHUNKS - 1:
-            for step in range(1, nz):
-                mine = xc.at[pd, piece_rows(k, (z - step + nz) % nz)]
-                arrived(mine, s_z.at[step], r_z.at[step])
-                go(remote(mine, mine, s_pair.at[step], r_pair.at[step], p, mate))
+
+    def wait_near(part):
         for at, other in enumerate((px, py)):
-            sem = 4 + 2 * chunk + at
-            arrived(xc.at[other, half_rows(1 - k, chunk)], s_pair.at[sem], r_pair.at[sem])
-        compute([(px, chunk * unit, unit), (py, chunk * unit, unit)])
-        if chunk == 0:
-            add_pair(p, 0)
-            add_pair(p, 1)
+            sem = 4 + 2 * part + at
+            arrived(xc.at[other, half_rows(1 - k, part)], s_pair.at[sem], r_pair.at[sem])
+
+    def compute_near(chunk):
+        lower, size = cuts[chunk], cuts[chunk + 1] - cuts[chunk]
+        compute([(px, lower, size), (py, lower, size)])
+
+    for at in range(width // 512):
+        for to in range(hidden_units // 256):
+            a, b = pl.ds(at * 512, 512), pl.ds(to * 256, 256)
+            wgt[b, a] = wg[a, b].T
+            wut[b, a] = wu[a, b].T
+            wdt[a, b] = wd[b, a].T
+    compute([(p, 0, rows)])
+    mine = xc.at[pd, piece_rows(k, z)]
+    arrived(mine, s_fwd.at[3], r_fwd.at[3])
+    for step in range(1, nz):
+        go(remote(mine, mine, s_z.at[step], r_z.at[step], p, (t + 2 * step) % n_tp))
+    go(remote(mine, mine, s_pair.at[0], r_pair.at[0], p, mate))
+    take_near(0)
+    for at, other in enumerate((px, py)):
+        passed = xc.at[other, sub_rows(k, at * piece, piece)]
+        sem = 4 + 2 * PARTS + at
+        go(remote(passed, passed, s_fwd.at[sem], r_fwd.at[sem], py if at == 0 else px, t))
+    send_near(2)
+    send_near(3)
+    for chunk in range(1, CHUNKS):
+        add_pair(p, chunk)
+    arrived(wt.at[pd], s_fwd.at[0], r_fwd.at[0])
+    arrived(wt.at[px], s_fwd.at[1], r_fwd.at[1])
+    arrived(wt.at[py], s_fwd.at[2], r_fwd.at[2])
+    wait_near(0)
+    compute_near(0)
+    take_near(1)
+    for step in range(1, nz):
+        mine = xc.at[pd, piece_rows(k, (z - step + nz) % nz)]
+        arrived(mine, s_z.at[step], r_z.at[step])
+        go(remote(mine, mine, s_pair.at[step], r_pair.at[step], p, mate))
+    z_first(p)
+    z_first(px)
+    z_first(py)
     for at in range(2):
-        sem = 4 + 2 * CHUNKS + at
+        sem = 4 + 2 * PARTS + at
         passed = xc.at[pd, sub_rows(k, at * piece, piece)]
         arrived(passed, s_fwd.at[sem], r_fwd.at[sem])
         go(remote(passed, passed, s_pair.at[sem], r_pair.at[sem], p, mate))
-    for chunk in range(CHUNKS):
-        first_near(chunk)
     for at in range(2):
-        sem = 4 + 2 * CHUNKS + at
+        sem = 4 + 2 * PARTS + at
         arrived(xc.at[pd, sub_rows(1 - k, at * piece, piece)], s_pair.at[sem], r_pair.at[sem])
     for step in range(nz):
         arrived(xc.at[pd, piece_rows(1 - k, (z - step + nz) % nz)], s_pair.at[step], r_pair.at[step])
     compute([(pd, 0, rows)])
-    for chunk in range(CHUNKS):
-        add_pair(pd, chunk)
-        for at in range(hz):
-            first(at, pd, 1, px, chunk)
-            first(hz + at, pd, 1, py, chunk)
-
-    for b in range(n_ep):
-        rm[b:b + 1, :] = rcol[b].T[0:1, :]
-    for step in range(1, n_tp):
-        go(remote(rm, rr.at[step], s_rt.at[step], r_rt.at[step], p, (t + step) % n_tp))
+    take_near(2)
+    first_pd(range(1, CHUNKS))
+    z_first(pd)
+    z_sum(p)
+    wait_near(1)
+    wait_near(2)
+    compute_near(1)
+    take_near(3)
+    z_sum(px)
+    z_sum(py)
+    first_near(1)
+    wait_near(3)
+    compute_near(2)
 
     def wide(ref, lower, count, cols):
         got = ref[:, pl.ds(lower, count), cols]
         return got.reshape(n_ep * count, got.shape[2])
 
-    def weight_grad(grads, out):
-        @pl.loop(0, width // 256)
-        def _(at):
-            cols = pl.ds(pl.multiple_of(at * 256, 256), 256)
-            out[cols, :] = lax.dot_general(
-                wide(xc, 0, rows, cols), wide(grads, 0, rows, slice(None)), tn, preferred_element_type=F32
+    def up_grads(*slices):
+        for at in slices:
+            cols = pl.ds(at * (width // 8), width // 8)
+            left = wide(xc, 0, rows, cols)
+            for grads, out in ((da, gg), (db, gu)):
+                out[cols, :] = lax.dot_general(
+                    left, wide(grads, 0, rows, slice(None)), tn, preferred_element_type=F32
+                ).astype(BF16)
+
+    def down_grads(*slices):
+        for at in slices:
+            cols = pl.ds(at * (width // 4), width // 4)
+            gd[:, cols] = lax.dot_general(
+                wide(hid, 0, rows, slice(None)), wide(sc, 0, rows, cols), tn, preferred_element_type=F32
             ).astype(BF16)
 
     def second(at, b, other, chunk):
-        span = pl.ds(chunk * unit, unit)
+        span = span_of(chunk)
         sem = xy_sem(at, 1, chunk)
         arrived(r1.at[at, 1, span], s_xy.at[sem], r_xy.at[sem])
         rp[k, at, b, span, :] = (rp[k, at, b, span, :].astype(F32) + r1[at, 1, span, :].astype(F32)).astype(BF16)
@@ -345,7 +410,7 @@
         go(remote(rp.at[k, at, b, span], r2.at[at, span], s_xy.at[sem], r_xy.at[sem], other, t))
 
     def third(chunk):
-        span = pl.ds(chunk * unit, unit)
+        span = span_of(chunk)
         for at in range(nz):
             for kind, ref in ((0, r1.at[at, 0, span]), (2, r2.at[at, span])):
                 sem = xy_sem(at, kind, chunk)
@@ -356,35 +421,39 @@
             sem = (1 + chunk) * nz + step
             go(remote(rp.at[k, (z + step) % nz, p, span], zr.at[step, span], s_z.at[sem], r_z.at[sem], p, (t + 2 * step) % n_tp))
 
-    for chunk in range(CHUNKS):
+    def second_both(chunk):
         for at in range(hz):
             second(at, py, py, chunk)
             second(hz + at, px, px, chunk)
 
-    total = rm[...]
-    for step in range(1, n_tp):
-        arrived(rr.at[step], s_rt.at[step], r_rt.at[step])
-        total = total + rr[step]
-    ra[...] = total
-    for at, other in enumerate((px, py, pd)):
-        go(remote(ra, rb.at[at], s_rt.at[n_tp + at], r_rt.at[n_tp + at], other, t))
-
-    weight_grad(da, gg)
-    third(0)
-    weight_grad(db, gu)
+    def send_route():
+        for b in range(n_ep):
+            rm[b:b + 1, :] = rcol[b].T[0:1, :]
+        for step in range(1, n_tp):
+            go(remote(rm, rr.at[step], s_rt.at[step], r_rt.at[step], p, (t + step) % n_tp))
+
+    def return_route():
+        total = rm[...]
+        for step in range(1, n_tp):
+            arrived(rr.at[step], s_rt.at[step], r_rt.at[step])
+            total = total + rr[step]
+        ra[...] = total
+        for at, other in enumerate((px, py, pd)):
+            go(remote(ra, rb.at[at], s_rt.at[n_tp + at], r_rt.at[n_tp + at], other, t))
+
+    second_both(1)
+    up_grads(0)
+    first_near(2)
+    second_both(2)
+    z_sum(pd)
+    send_route()
+    up_grads(1, 2)
     third(1)
-
-    @pl.loop(0, hidden_units // 256)
-    def _(at):
-        units = pl.ds(pl.multiple_of(at * 256, 256), 256)
-        left = wide(hid, 0, rows, units)
-
-        @pl.loop(0, width // 512)
-        def _(to):
-            cols = pl.ds(pl.multiple_of(to * 512, 512), 512)
-            gd[units, cols] = lax.dot_general(
-                left, wide(sc, 0, rows, cols), tn, preferred_element_type=F32
-            ).astype(BF16)
+    up_grads(3, 4)
+    return_route()
+    third(2)
+    up_grads(5, 6, 7)
+    down_grads(0, 1, 2, 3)
 
     index = lax.broadcasted_iota(jnp.int32, rm.shape, 0)
     result = jnp.zeros(rm.shape, F32)
@@ -398,13 +467,19 @@
         hit = routes_ref[choice:choice + 1, :] == experts
         rt_ref[choice:choice + 1, :] = jnp.sum(jnp.where(hit, result[:, 0:rows], 0.0), axis=0, keepdims=True)
 
-    total = rp[k, z, p].astype(F32)
-    for step in range(1, nz):
-        for chunk in range(CHUNKS):
+    total = rp[k, z, p, span_of(0), :].astype(F32)
+    for at in range(3):
+        arrived(rq.at[at], s_rq.at[at], r_rq.at[at])
+        total = total + rq[at].astype(F32)
+    gt_ref[span_of(0), :] = total.astype(BF16)
+    for chunk in range(1, CHUNKS):
+        span = span_of(chunk)
+        total = rp[k, z, p, span, :].astype(F32)
+        for step in range(1, nz):
             sem = (1 + chunk) * nz + step
-            arrived(zr.at[step, pl.ds(chunk * unit, unit)], s_z.at[sem], r_z.at[sem])
-        total = total + zr[step].astype(F32)
-    gt_ref[...] = total.astype(BF16)
+            arrived(zr.at[step, span], s_z.at[sem], r_z.at[sem])
+            total = total + zr[step, span, :].astype(F32)
+        gt_ref[span, :] = total.astype(BF16)
     for copy in sends:
         copy.wait_send()
 
@@ -439,6 +514,9 @@
         scratch_shapes=[
             pltpu.VMEM((routes.shape[1], rows), jnp.int32),
             pltpu.VMEM((routes.shape[1], rows), F32),
+            pltpu.VMEM((units, width), BF16),
+            pltpu.VMEM((units, width), BF16),
+            pltpu.VMEM((width, units), BF16),
             pltpu.VMEM((n_ep, 2 * rows, width), BF16),
             pltpu.VMEM((n_ep, 8, LANES), F32),
             pltpu.VMEM((width, units), BF16),
@@ -458,11 +536,17 @@
             pltpu.VMEM((n_tp, 8, LANES), F32),
             pltpu.VMEM((8, LANES), F32),
             pltpu.VMEM((3, 8, LANES), F32),
+            pltpu.VMEM((nz, n_ep, 2 * (rows // (nz + 2)), shard), BF16),
+            pltpu.VMEM((3, 2 * (rows // (nz + 2)), shard), BF16),
+            dma((n_ep * nz,)),
+            dma((n_ep * nz,)),
+            dma((3,)),
+            dma((3,)),
             dma((7,)),
-            dma((6 + 2 * CHUNKS,)),
-            dma((6 + 2 * CHUNKS,)),
-            dma((6 + 2 * CHUNKS,)),
-            dma((6 + 2 * CHUNKS,)),
+            dma((6 + 2 * PARTS,)),
+            dma((6 + 2 * PARTS,)),
+            dma((6 + 2 * PARTS,)),
+            dma((6 + 2 * PARTS,)),
             dma((n_ep * CHUNKS,)),
             dma((n_ep * CHUNKS,)),
             dma((3 * nz * CHUNKS,)),
@@ -499,7 +583,7 @@
     fits = (
         n_ep == 4 and experts == 1 and n_tp == 8 and capacity >= rows and rows <= LANES
         and width % (n_tp * 128) == 0 and width % 512 == 0 and units % 256 == 0
-        and rows % (16 * (n_tp // 2 + 2)) == 0 and 2 * (rows // (n_tp // 2 + 2)) <= rows // CHUNKS and rows % (16 * CHUNKS) == 0
+        and units >= 512 and width % 1024 == 0 and rows % (16 * (n_tp // 2 + 2)) == 0
     )
     return fused(n_ep, n_tp, *arrays) if fits else shards(*arrays)
 

time: 63.3 us -> 54.5 us (0.86)
  Pallas kernels: 62.4 us -> 53.6 us
    pallas_call x1, Pallas kernels: 59.6 us -> 50.8 us  [fused(): pl.pallas_call(functools.partial(step_kernel, n_ep, n_tp), out_shape=(jax...]
where the time goes in v2:
time: 54.5 us; the launch traced here: 54.4 us
  Pallas kernels  53.6 us (98%)
  between operations  0.8 us (1%)
    pallas_call x1, Pallas kernels, fused(): pl.pallas_call(functools.partial(step_kernel, n_ep, n_tp), out_shape=(jax...  50.8 us
    pallas_call x1, Pallas kernels, fused(): pl.pallas_call(write_kernel, out_shape=tuple((jax.ShapeDtypeStruct(array....  2.78 us

profile of v2, /device:TPU:0, one launch (start us, length us, event | category | flops | bytes accessed | tf_op | source)
XLA Modules:
  0.0 54.4 jit_solution(15633231744647070056)
XLA Ops:
  0.6 50.8 %shard_map.110 = (bf16[192,256]{1,0:T(8,128)(2,1)S(1)}, f32[2,192]{1,0:T(2,128)S(1)}, bf16[2048,512]{1,0:T(8,128)(2,1)S(1)}, bf16[2048,512]{1,0:T(8,128)(2,1)S(1)}, bf16[512,2048]{1,0:T(8,128)(2,1)S(1)}) custom-call(bf16[192,2048]{1,0:T(8,128)(2,1)} %x_hbm.1, bf16[192,2048]{1,0:T(8,128)(2,1)} %c_hbm.1, s32[2,192]{1,0:T(2,128)} %bitcast.12, ...), custom_call_target="tpu_custom_call" | custom-call | tf_op jit(solution)/shard_map/pallas_call | solution.py:503
  51.4 2.8 %shard_map.111 = (bf16[192,256]{1,0:T(8,128)(2,1)}, f32[2,192]{1,0:T(2,128)}, bf16[2048,512]{1,0:T(8,128)(2,1)}, bf16[2048,512]{1,0:T(8,128)(2,1)}, bf16[512,2048]{1,0:T(8,128)(2,1)}) custom-call(bf16[192,256]{1,0:T(8,128)(2,1)S(1)} %get-tuple-element.15.refs_0_, f32[2,192]{1,0:T(2,128)S(1)} %get-tuple-element.16.refs_1_, ...), custom_call_target="tpu_custom_call" | custom-call | tf_op jit(solution)/shard_map/pallas_call | solution.py:566

commit v3 on v2

--- a/solution.py
+++ b/solution.py
@@ -9,7 +9,7 @@
 
 F32, BF16 = jnp.float32, jnp.bfloat16
 LANES = 256
-CHUNKS = 3
+CHUNKS = 4
 PARTS = 4
 VLIM = 40
 
@@ -108,8 +108,8 @@
 def step_kernel(
     n_ep, n_tp,
     x_hbm, c_hbm, routes_hbm, weight_hbm, wg_hbm, wu_hbm, wd_hbm,
-    gt_ref, rt_ref, gg, gu, gd,
-    routes_ref, weight_ref, wgt, wut, wdt, xc, wt, wg, wu, wd, hid, da, db, sc, rp, pr, r1, r2, zr, rcol, rm, rr, ra, rb,
+    gt_ref, rt_ref, gg, gu, hid, sc,
+    routes_ref, weight_ref, wgt, wut, wdt, xc, wt, wg, wu, wd, da, db, rp, pr, r1, r2, zr, rcol, rm, rr, ra, rb,
     zq, rq, s_zf, r_zf, s_rq, r_rq, lsem, s_fwd, r_fwd, s_pair, r_pair, s_rp, r_rp, s_xy, r_xy, s_z, r_z, s_rt, r_rt,
 ):
     nz = n_tp // 2
@@ -118,9 +118,9 @@
     hidden_units = wg.shape[1]
     shard = width // n_tp
     piece = rows // (nz + 2)
-    cuts = (0, 2 * piece, rows - piece, rows)
-    middle = 2 * piece + (rows - 3 * piece) // 32 * 16
-    ends = (0, 2 * piece, middle, rows - piece, rows)
+    ends = (0, 2 * piece, 3 * piece, 4 * piece, rows)
+    groups = ((0, 2 * piece), (2 * piece, 2 * piece), (4 * piece, rows - 4 * piece))
+    cuts = (0, 2 * piece, 4 * piece, rows - piece, rows)
     p, t = lax.axis_index("ep"), lax.axis_index("tp")
     k, z = t % 2, t // 2
     px, py, pd = p + 1 - 2 * (p % 2), p + 2 - 4 * (p // 2), 3 - p
@@ -205,7 +205,7 @@
         row = jnp.sum(jnp.where(at_expert, wt[b], 0.0), axis=0, keepdims=True)
         return jnp.broadcast_to(row, (128, LANES)).T[:, 0:1]
 
-    def compute(parts):
+    def compute(parts, between=None):
         count = sum(size for _, _, size in parts)
 
         def load(ref, shift, cols):
@@ -222,7 +222,7 @@
         weight = [weights_of(b)[lower:lower + size] for b, lower, size in parts]
         weight = weight[0] if len(weight) == 1 else jnp.concatenate(weight, axis=0)
         tile = min(hidden_units, 256)
-        route = jnp.zeros((count, 1), F32)
+        route, das, dbs = jnp.zeros((count, 1), F32), [], []
         for at in range(hidden_units // tile):
             cols = pl.ds(at * tile, tile)
             x = load(xc, 0, every)
@@ -235,13 +235,21 @@
             store(hid, cols, hidden)
             route = route + jnp.sum(hidden.astype(F32) * back, axis=1, keepdims=True)
             scaled = weight * back
-            store(da, cols, (scaled * up * sig * (1.0 + gate * (1.0 - sig))).astype(BF16))
-            store(db, cols, (scaled * active).astype(BF16))
+            das.append((scaled * up * sig * (1.0 + gate * (1.0 - sig))).astype(BF16))
+            dbs.append((scaled * active).astype(BF16))
+            store(da, cols, das[-1])
+            store(db, cols, dbs[-1])
         store(rcol, every, jnp.broadcast_to(route, (count, 128)))
+        if between is not None:
+            between()
         for at in range(nz):
             cols = pl.ds(2 * at * shard, 2 * shard)
-            part = jnp.dot(load(da, 0, every), wgt[:, cols], preferred_element_type=F32)
-            part = part + jnp.dot(load(db, 0, every), wut[:, cols], preferred_element_type=F32)
+            part = None
+            for up_to, (left, right) in enumerate(zip(das, dbs)):
+                units = pl.ds(up_to * tile, tile)
+                term = jnp.dot(left, wgt[units, cols], preferred_element_type=F32)
+                part = term if part is None else part + term
+                part = part + jnp.dot(right, wut[units, cols], preferred_element_type=F32)
             part, done = part.astype(BF16), 0
             for b, lower, size in parts:
                 for core in range(2):
@@ -306,6 +314,14 @@
                 first(at, pd, 1, px, chunk)
                 first(hz + at, pd, 1, py, chunk)
 
+    def second(at, b, other, chunk):
+        span = span_of(chunk)
+        sem = xy_sem(at, 1, chunk)
+        arrived(r1.at[at, 1, span], s_xy.at[sem], r_xy.at[sem])
+        rp[k, at, b, span, :] = (rp[k, at, b, span, :].astype(F32) + r1[at, 1, span, :].astype(F32)).astype(BF16)
+        sem = xy_sem(at, 2, chunk)
+        go(remote(rp.at[k, at, b, span], r2.at[at, span], s_xy.at[sem], r_xy.at[sem], other, t))
+
     def take_near(part):
         for at, other in enumerate((px, py)):
             mine = xc.at[other, half_rows(k, part)]
@@ -318,9 +334,9 @@
             sem = 4 + 2 * part + at
             arrived(xc.at[other, half_rows(1 - k, part)], s_pair.at[sem], r_pair.at[sem])
 
-    def compute_near(chunk):
-        lower, size = cuts[chunk], cuts[chunk + 1] - cuts[chunk]
-        compute([(px, lower, size), (py, lower, size)])
+    def compute_near(group, between=None):
+        lower, size = groups[group]
+        compute([(px, lower, size), (py, lower, size)], between)
 
     for at in range(width // 512):
         for to in range(hidden_units // 256):
@@ -353,33 +369,39 @@
         mine = xc.at[pd, piece_rows(k, (z - step + nz) % nz)]
         arrived(mine, s_z.at[step], r_z.at[step])
         go(remote(mine, mine, s_pair.at[step], r_pair.at[step], p, mate))
+    for at in range(2):
+        sem = 4 + 2 * PARTS + at
+        passed = xc.at[pd, sub_rows(k, at * piece, piece)]
+        arrived(passed, s_fwd.at[sem], r_fwd.at[sem])
+        go(remote(passed, passed, s_pair.at[sem], r_pair.at[sem], p, mate))
     z_first(p)
     z_first(px)
     z_first(py)
     for at in range(2):
         sem = 4 + 2 * PARTS + at
-        passed = xc.at[pd, sub_rows(k, at * piece, piece)]
-        arrived(passed, s_fwd.at[sem], r_fwd.at[sem])
-        go(remote(passed, passed, s_pair.at[sem], r_pair.at[sem], p, mate))
-    for at in range(2):
-        sem = 4 + 2 * PARTS + at
         arrived(xc.at[pd, sub_rows(1 - k, at * piece, piece)], s_pair.at[sem], r_pair.at[sem])
     for step in range(nz):
         arrived(xc.at[pd, piece_rows(1 - k, (z - step + nz) % nz)], s_pair.at[step], r_pair.at[step])
-    compute([(pd, 0, rows)])
-    take_near(2)
-    first_pd(range(1, CHUNKS))
-    z_first(pd)
-    z_sum(p)
+    compute([(pd, 0, rows)], lambda: take_near(2))
     wait_near(1)
     wait_near(2)
-    compute_near(1)
+
+    def send_far():
+        first_pd(range(1, CHUNKS))
+        z_first(pd)
+
+    compute_near(1, send_far)
+    z_sum(p)
     take_near(3)
-    z_sum(px)
-    z_sum(py)
     first_near(1)
+
+    def second_both(chunk):
+        for at in range(hz):
+            second(at, py, py, chunk)
+            second(hz + at, px, px, chunk)
+
     wait_near(3)
-    compute_near(2)
+    compute_near(2, lambda: second_both(1))
 
     def wide(ref, lower, count, cols):
         got = ref[:, pl.ds(lower, count), cols]
@@ -393,21 +415,6 @@
                 out[cols, :] = lax.dot_general(
                     left, wide(grads, 0, rows, slice(None)), tn, preferred_element_type=F32
                 ).astype(BF16)
-
-    def down_grads(*slices):
-        for at in slices:
-            cols = pl.ds(at * (width // 4), width // 4)
-            gd[:, cols] = lax.dot_general(
-                wide(hid, 0, rows, slice(None)), wide(sc, 0, rows, cols), tn, preferred_element_type=F32
-            ).astype(BF16)
-
-    def second(at, b, other, chunk):
-        span = span_of(chunk)
-        sem = xy_sem(at, 1, chunk)
-        arrived(r1.at[at, 1, span], s_xy.at[sem], r_xy.at[sem])
-        rp[k, at, b, span, :] = (rp[k, at, b, span, :].astype(F32) + r1[at, 1, span, :].astype(F32)).astype(BF16)
-        sem = xy_sem(at, 2, chunk)
-        go(remote(rp.at[k, at, b, span], r2.at[at, span], s_xy.at[sem], r_xy.at[sem], other, t))
 
     def third(chunk):
         span = span_of(chunk)
@@ -421,11 +428,6 @@
             sem = (1 + chunk) * nz + step
             go(remote(rp.at[k, (z + step) % nz, p, span], zr.at[step, span], s_z.at[sem], r_z.at[sem], p, (t + 2 * step) % n_tp))
 
-    def second_both(chunk):
-        for at in range(hz):
-            second(at, py, py, chunk)
-            second(hz + at, px, px, chunk)
-
     def send_route():
         for b in range(n_ep):
             rm[b:b + 1, :] = rcol[b].T[0:1, :]
@@ -441,19 +443,23 @@
         for at, other in enumerate((px, py, pd)):
             go(remote(ra, rb.at[at], s_rt.at[n_tp + at], r_rt.at[n_tp + at], other, t))
 
-    second_both(1)
-    up_grads(0)
-    first_near(2)
-    second_both(2)
+    send_route()
+    up_grads(0, 1)
+    for chunk in range(2, CHUNKS):
+        first_near(chunk)
+        second_both(chunk)
+    third(1)
+    up_grads(2, 3)
+    z_sum(px)
+    z_sum(py)
     z_sum(pd)
-    send_route()
-    up_grads(1, 2)
-    third(1)
-    up_grads(3, 4)
+    up_grads(4)
     return_route()
+    up_grads(5)
     third(2)
-    up_grads(5, 6, 7)
-    down_grads(0, 1, 2, 3)
+    up_grads(6)
+    third(3)
+    up_grads(7)
 
     index = lax.broadcasted_iota(jnp.int32, rm.shape, 0)
     result = jnp.zeros(rm.shape, F32)
@@ -484,11 +490,21 @@
         copy.wait_send()
 
 
-def write_kernel(*refs):
-    sem = refs[-1]
-    copies = [pltpu.make_async_copy(refs[at], refs[5 + at], sem.at[at]) for at in range(5)]
+def write_kernel(gt, rt, gg, gu, hid, sc, gt_hbm, rt_hbm, gg_hbm, gu_hbm, gd_hbm, gd, sem):
+    pairs = ((gt, gt_hbm), (rt, rt_hbm), (gg, gg_hbm), (gu, gu_hbm))
+    copies = [pltpu.make_async_copy(left, right, sem.at[at]) for at, (left, right) in enumerate(pairs)]
+    units, width = gd.shape
+    merged = hid.shape[0] * hid.shape[1]
     for copy in copies:
         copy.start()
+    for at in range(4):
+        cols = pl.ds(at * (width // 4), width // 4)
+        gd[:, cols] = lax.dot_general(
+            hid[...].reshape(merged, units), sc[:, :, cols].reshape(merged, width // 4),
+            (((0,), (0,)), ((), ())), preferred_element_type=F32,
+        ).astype(BF16)
+        copies.append(pltpu.make_async_copy(gd.at[:, cols], gd_hbm.at[:, cols], sem.at[4 + at]))
+        copies[-1].start()
     for copy in copies:
         copy.wait()
 
@@ -500,17 +516,18 @@
     shard = width // n_tp
     hbm, vmem = pl.BlockSpec(memory_space=pltpu.HBM), pl.BlockSpec(memory_space=pltpu.VMEM)
     dma = pltpu.SemaphoreType.DMA
-    grad_tokens, by_choice, grad_gate, grad_up, grad_down = pl.pallas_call(
+    results = pl.pallas_call(
         functools.partial(step_kernel, n_ep, n_tp),
         out_shape=(
             jax.ShapeDtypeStruct((rows, shard), BF16),
             jax.ShapeDtypeStruct((routes.shape[1], rows), F32),
             jax.ShapeDtypeStruct((width, units), BF16),
             jax.ShapeDtypeStruct((width, units), BF16),
-            jax.ShapeDtypeStruct((units, width), BF16),
+            jax.ShapeDtypeStruct((n_ep, rows, units), BF16),
+            jax.ShapeDtypeStruct((n_ep, rows, width), BF16),
         ),
         in_specs=[hbm] * 7,
-        out_specs=(vmem,) * 5,
+        out_specs=(vmem,) * 6,
         scratch_shapes=[
             pltpu.VMEM((routes.shape[1], rows), jnp.int32),
             pltpu.VMEM((routes.shape[1], rows), F32),
@@ -524,8 +541,6 @@
             pltpu.VMEM((units, width), BF16),
             pltpu.VMEM((n_ep, rows, units), BF16),
             pltpu.VMEM((n_ep, rows, units), BF16),
-            pltpu.VMEM((n_ep, rows, units), BF16),
-            pltpu.VMEM((n_ep, rows, width), BF16),
             pltpu.VMEM((2, nz, n_ep, rows, shard), BF16),
             pltpu.VMEM((nz, n_ep, rows, shard), BF16),
             pltpu.VMEM((nz, 2, rows, shard), BF16),
@@ -562,14 +577,14 @@
     )(*(pltpu.with_memory_space_constraint(array, pltpu.HBM) for array in (
         tokens, cotangent, routes.T, route_weight.T, gate_weight[0], up_weight[0], down_weight[0]
     )))
-    results = (grad_tokens, by_choice, grad_gate, grad_up, grad_down)
     grad_tokens, by_choice, grad_gate, grad_up, grad_down = pl.pallas_call(
         write_kernel,
-        out_shape=tuple(jax.ShapeDtypeStruct(array.shape, array.dtype) for array in results),
-        in_specs=[vmem] * 5,
+        out_shape=tuple(jax.ShapeDtypeStruct(array.shape, array.dtype) for array in results[:4])
+        + (jax.ShapeDtypeStruct((units, width), BF16),),
+        in_specs=[vmem] * 6,
         out_specs=(hbm,) * 5,
-        scratch_shapes=[dma((5,))],
-        compiler_params=pltpu.CompilerParams(vmem_limit_bytes=1024 * 1024),
+        scratch_shapes=[pltpu.VMEM((units, width), BF16), dma((8,))],
+        compiler_params=pltpu.CompilerParams(vmem_limit_bytes=8 * 1024 * 1024),
     )(*results)
     grad_route = by_choice.T
     return grad_tokens, grad_route, grad_gate[None], grad_up[None], grad_down[None]

time: 54.5 us -> 51.7 us (0.949)
  Pallas kernels: 53.6 us -> 50.7 us
    pallas_call x1, Pallas kernels: 50.8 us -> 48 us  [fused(): pl.pallas_call(functools.partial(step_kernel, n_ep, n_tp), out_shape=(jax...]
where the time goes in v3:
time: 51.7 us; the launch traced here: 51.5 us
  Pallas kernels  50.7 us (98%)
  between operations  0.8 us (2%)
    pallas_call x1, Pallas kernels, fused(): pl.pallas_call(functools.partial(step_kernel, n_ep, n_tp), out_shape=(jax...  48 us
    pallas_call x1, Pallas kernels, fused(): pl.pallas_call(write_kernel, out_shape=tuple((jax.ShapeDtypeStruct(array....  2.76 us

profile of v3, /device:TPU:0, one launch (start us, length us, event | category | flops | bytes accessed | tf_op | source)
XLA Modules:
  0.0 51.5 jit_solution(6367926863300745411)
XLA Ops:
  0.6 48.0 %shard_map.110 = (bf16[192,256]{1,0:T(8,128)(2,1)S(1)}, f32[2,192]{1,0:T(2,128)S(1)}, bf16[2048,512]{1,0:T(8,128)(2,1)S(1)}, bf16[2048,512]{1,0:T(8,128)(2,1)S(1...) custom-call(bf16[192,2048]{1,0:T(8,128)(2,1)} %x_hbm.1, bf16[192,2048]{1,0:T(8,128)(2,1)} %c_hbm.1, ...), custom_call_target="tpu_custom_call" | custom-call | tf_op jit(solution)/shard_map/pallas_call | solution.py:519
  48.6 2.8 %shard_map.111 = (bf16[192,256]{1,0:T(8,128)(2,1)}, f32[2,192]{1,0:T(2,128)}, bf16[2048,512]{1,0:T(8,128)(2,1)}, bf16[2048,512]{1,0:T(8,128)(2,1)}, bf16[512,2048]{1,0:T(8,128)(2,1)}) custom-call(bf16[192,256]{1,0:T(8,128)(2,1)S(1)} %get-tuple-element.16.gt, f32[2,192]{1,0:T(2,128)S(1)} %get-tuple-element.17.rt, bf16[2048,512]{1,0:T(8,128)(2,1)S(1)} %get-tuple-element.18.gg, ...), custom_call_target="tpu_custom_call" | custom-call | tf_op jit(solution)/shard_map/pallas_call | solution.py:580

commit v4 on v3

--- a/solution.py
+++ b/solution.py
@@ -181,13 +181,13 @@
 
     for at, other in enumerate((pd, px, py)):
         go(remote(wt.at[p], wt.at[p], s_fwd.at[at], r_fwd.at[at], other, t))
-    mine = xc.at[p, piece_rows(k, z)]
+    mine = xc.at[p, piece_rows(1 - k, z)]
     go(remote(mine, mine, s_fwd.at[3], r_fwd.at[3], pd, t))
 
     def send_near(part):
         for at, other in enumerate((px, py)):
             sem = 4 + 2 * part + at
-            mine = xc.at[p, half_rows(k, part)]
+            mine = xc.at[p, half_rows(1 - k, part)]
             go(remote(mine, mine, s_fwd.at[sem], r_fwd.at[sem], other, t))
 
     send_near(0)
@@ -324,7 +324,7 @@
 
     def take_near(part):
         for at, other in enumerate((px, py)):
-            mine = xc.at[other, half_rows(k, part)]
+            mine = xc.at[other, half_rows(1 - k, part)]
             sem = 4 + 2 * part + at
             arrived(mine, s_fwd.at[sem], r_fwd.at[sem])
             go(remote(mine, mine, s_pair.at[sem], r_pair.at[sem], p, mate))
@@ -332,7 +332,7 @@
     def wait_near(part):
         for at, other in enumerate((px, py)):
             sem = 4 + 2 * part + at
-            arrived(xc.at[other, half_rows(1 - k, part)], s_pair.at[sem], r_pair.at[sem])
+            arrived(xc.at[other, half_rows(k, part)], s_pair.at[sem], r_pair.at[sem])
 
     def compute_near(group, between=None):
         lower, size = groups[group]
@@ -345,14 +345,14 @@
             wut[b, a] = wu[a, b].T
             wdt[a, b] = wd[b, a].T
     compute([(p, 0, rows)])
-    mine = xc.at[pd, piece_rows(k, z)]
+    mine = xc.at[pd, piece_rows(1 - k, z)]
     arrived(mine, s_fwd.at[3], r_fwd.at[3])
     for step in range(1, nz):
         go(remote(mine, mine, s_z.at[step], r_z.at[step], p, (t + 2 * step) % n_tp))
     go(remote(mine, mine, s_pair.at[0], r_pair.at[0], p, mate))
     take_near(0)
     for at, other in enumerate((px, py)):
-        passed = xc.at[other, sub_rows(k, at * piece, piece)]
+        passed = xc.at[other, sub_rows(1 - k, at * piece, piece)]
         sem = 4 + 2 * PARTS + at
         go(remote(passed, passed, s_fwd.at[sem], r_fwd.at[sem], py if at == 0 else px, t))
     send_near(2)
@@ -366,23 +366,27 @@
     compute_near(0)
     take_near(1)
     for step in range(1, nz):
-        mine = xc.at[pd, piece_rows(k, (z - step + nz) % nz)]
+        mine = xc.at[pd, piece_rows(1 - k, (z - step + nz) % nz)]
         arrived(mine, s_z.at[step], r_z.at[step])
         go(remote(mine, mine, s_pair.at[step], r_pair.at[step], p, mate))
     for at in range(2):
         sem = 4 + 2 * PARTS + at
-        passed = xc.at[pd, sub_rows(k, at * piece, piece)]
+        passed = xc.at[pd, sub_rows(1 - k, at * piece, piece)]
         arrived(passed, s_fwd.at[sem], r_fwd.at[sem])
         go(remote(passed, passed, s_pair.at[sem], r_pair.at[sem], p, mate))
-    z_first(p)
     z_first(px)
     z_first(py)
     for at in range(2):
         sem = 4 + 2 * PARTS + at
-        arrived(xc.at[pd, sub_rows(1 - k, at * piece, piece)], s_pair.at[sem], r_pair.at[sem])
+        arrived(xc.at[pd, sub_rows(k, at * piece, piece)], s_pair.at[sem], r_pair.at[sem])
     for step in range(nz):
-        arrived(xc.at[pd, piece_rows(1 - k, (z - step + nz) % nz)], s_pair.at[step], r_pair.at[step])
-    compute([(pd, 0, rows)], lambda: take_near(2))
+        arrived(xc.at[pd, piece_rows(k, (z - step + nz) % nz)], s_pair.at[step], r_pair.at[step])
+
+    def pass_on():
+        take_near(2)
+        z_first(p)
+
+    compute([(pd, 0, rows)], pass_on)
     wait_near(1)
     wait_near(2)
 
@@ -391,7 +395,6 @@
         z_first(pd)
 
     compute_near(1, send_far)
-    z_sum(p)
     take_near(3)
     first_near(1)
 
@@ -450,16 +453,16 @@
         second_both(chunk)
     third(1)
     up_grads(2, 3)
+    z_sum(p)
     z_sum(px)
     z_sum(py)
     z_sum(pd)
     up_grads(4)
+    third(2)
+    up_grads(5)
+    third(3)
     return_route()
-    up_grads(5)
-    third(2)
-    up_grads(6)
-    third(3)
-    up_grads(7)
+    up_grads(6, 7)
 
     index = lax.broadcasted_iota(jnp.int32, rm.shape, 0)
     result = jnp.zeros(rm.shape, F32)

time: 51.7 us -> 51.6 us (level)
  no operation moved by 1% of the time
where the time goes in v4:
time: 51.6 us; the launch traced here: 51.4 us
  Pallas kernels  50.6 us (98%)
  between operations  0.8 us (2%)
    pallas_call x1, Pallas kernels, fused(): pl.pallas_call(functools.partial(step_kernel, n_ep, n_tp), out_shape=(jax...  47.8 us
    pallas_call x1, Pallas kernels, fused(): pl.pallas_call(write_kernel, out_shape=tuple((jax.ShapeDtypeStruct(array....  2.76 us

profile of v4, /device:TPU:0, one launch (start us, length us, event | category | flops | bytes accessed | tf_op | source)
XLA Modules:
  0.0 51.4 jit_solution(16973715904547676888)
XLA Ops:
  0.6 47.8 %shard_map.110 = (bf16[192,256]{1,0:T(8,128)(2,1)S(1)}, f32[2,192]{1,0:T(2,128)S(1)}, bf16[2048,512]{1,0:T(8,128)(2,1)S(1)}, bf16[2048,512]{1,0:T(8,128)(2,1)S(1...) custom-call(bf16[192,2048]{1,0:T(8,128)(2,1)} %x_hbm.1, bf16[192,2048]{1,0:T(8,128)(2,1)} %c_hbm.1, ...), custom_call_target="tpu_custom_call" | custom-call | tf_op jit(solution)/shard_map/pallas_call | solution.py:522
  48.5 2.8 %shard_map.111 = (bf16[192,256]{1,0:T(8,128)(2,1)}, f32[2,192]{1,0:T(2,128)}, bf16[2048,512]{1,0:T(8,128)(2,1)}, bf16[2048,512]{1,0:T(8,128)(2,1)}, bf16[512,2048]{1,0:T(8,128)(2,1)}) custom-call(bf16[192,256]{1,0:T(8,128)(2,1)S(1)} %get-tuple-element.16.gt, f32[2,192]{1,0:T(2,128)S(1)} %get-tuple-element.17.rt, bf16[2048,512]{1,0:T(8,128)(2,1)S(1)} %get-tuple-element.18.gg, ...), custom_call_target="tpu_custom_call" | custom-call | tf_op jit(solution)/shard_map/pallas_call | solution.py:583
